TPU v7x, 32 devices: a whole 2x2x4 slice. The times are simulated.
32 devices in a mesh: ep: 4 (over y, x), tp: 8 (over z, core).
Axes of the slice: x: 2, y: 2, z: 4, core: 2. Of those that a mesh axis runs over, the one named last changes fastest.
Arguments:
- hidden_in: bfloat16 [128, 4096], P('ep'), may hold values from -6 to 6
- mix_gain: float32 [4096], replicated, may hold values from 0.1 to 1.9
- w_query: bfloat16 [4096, 2048], P('ep', 'tp'), may hold values from -0.09375 to 0.09375
- w_key: bfloat16 [4096, 2048], P('ep', 'tp'), may hold values from -0.09375 to 0.09375
- w_value: bfloat16 [4096, 2048], P('ep', 'tp'), may hold values from -0.09375 to 0.09375
- w_outgate: bfloat16 [4096, 2048], P('ep', 'tp'), may hold values from -0.09375 to 0.09375
- w_gates: bfloat16 [2, 4096, 32], P(None, None, 'tp'), may hold values from -0.09375 to 0.09375
- gate_bias: float32 [2, 32], P(None, 'tp'), may hold values from -1 to 4
- state_matrix: float32 [128, 32, 64, 64], P('ep', 'tp'), may hold values from -2 to 2
- state_norm: float32 [128, 32, 64], P('ep', 'tp'), may hold values from -2 to 2
- state_max: float32 [128, 32], P('ep', 'tp'), may hold values from -3 to 3
- w_mix_out: bfloat16 [2048, 4096], P('tp'), may hold values from -0.125 to 0.125
- ffn_gain: float32 [4096], replicated, may hold values from 0.1 to 1.9
- routes: int32 [128, 2], replicated, may hold values from 0 to 7, all different within a row; in each aligned block of 32 rows (0 to 31, 32 to 63, ...) at most 9 rows name the same one
- route_weights: float32 [128, 2], P('ep'), may hold values from 0.1 to 1
- expert_gate: bfloat16 [8, 4096, 2048], P('ep', None, 'tp'), may hold values from -0.09375 to 0.09375
- expert_up: bfloat16 [8, 4096, 2048], P('ep', None, 'tp'), may hold values from -0.09375 to 0.09375
- expert_down: bfloat16 [8, 2048, 4096], P('ep', 'tp'), may hold values from -0.125 to 0.125
- shared_gate: bfloat16 [4096, 1024], P(None, 'tp'), may hold values from -0.09375 to 0.09375
- shared_up: bfloat16 [4096, 1024], P(None, 'tp'), may hold values from -0.09375 to 0.09375
- shared_down: bfloat16 [1024, 4096], P('tp'), may hold values from -0.1875 to 0.1875
Outputs:
- result: bfloat16 [128, 4096], P('ep', 'tp')
- new_matrix: float32 [128, 32, 64, 64], P('ep', 'tp')
- new_norm: float32 [128, 32, 64], P('ep', 'tp')
- new_max: float32 [128, 32], P('ep', 'tp')
Inputs may be any that keep to these rules, and one draw needn't show every extreme that they name: `routes`: each row names 2 different experts. In each aligned block of 32 rows (the rows of one device group along ep) no expert is named by more than 9 rows, a bound that some block reaches.
All inputs are finite; a program needn't handle non-finite values.
Results may differ from a plain program's by a relative error of at most 0.023.
Values may be sent and summed in bfloat16 or wider, within the bound.
A program may use at most 64 MiB of HBM per device.

v0:
```python
import jax
import jax.numpy as jnp
from jax import lax
from jax.sharding import PartitionSpec as P

norm_eps = 1e-06


def rms_scale(inputs, scales):
    floats = inputs.astype(jnp.float32)
    return floats * lax.rsqrt(jnp.mean(floats * floats, -1, keepdims=True) + norm_eps) * scales


def slot_ranks(chosen, experts):
    flat_ids = chosen.reshape(-1)
    onehot = (flat_ids[:, None] == jnp.arange(experts, dtype=jnp.int32)[None, :]).astype(jnp.int32)
    earlier = jnp.cumsum(onehot, 0) - onehot
    return jnp.sum(earlier * onehot, 1).reshape(chosen.shape)


def per_device(
    hidden_in,
    mix_gain,
    w_query,
    w_key,
    w_value,
    w_outgate,
    w_gates,
    gate_bias,
    state_matrix,
    state_norm,
    state_max,
    w_mix_out,
    ffn_gain,
    routes,
    route_weights,
    expert_gate,
    expert_up,
    expert_down,
    shared_gate,
    shared_up,
    shared_down,
):
    ep_count = lax.axis_size("ep")
    tp_count = lax.axis_size("tp")
    group_index = lax.axis_index("ep")
    column_index = lax.axis_index("tp")
    seq_rows, width = hidden_in.shape
    heads_dev = state_matrix.shape[1]
    head_dim = state_matrix.shape[2]
    top_count = routes.shape[1]
    local_experts = expert_gate.shape[0]
    expert_total = local_experts * ep_count
    capacity = max(2, seq_rows * top_count // expert_total + 1)
    slot_count = ep_count * capacity
    slice_width = width // tp_count
    normed = rms_scale(hidden_in, mix_gain).astype(jnp.bfloat16)
    gathered = lax.all_to_all(normed, "ep", split_axis=1, concat_axis=0, tiled=True)
    joined = jnp.concatenate([w_query, w_key, w_value, w_outgate], 1)
    projected = lax.psum_scatter(
        jnp.dot(gathered, joined, preferred_element_type=jnp.float32).astype(jnp.bfloat16),
        "ep",
        scatter_dimension=0,
        tiled=True,
    )
    head_cols = heads_dev * head_dim

    def heads_of(role_index):
        part = projected[:, role_index * head_cols : (role_index + 1) * head_cols]
        return part.astype(jnp.float32).reshape(seq_rows, heads_dev, head_dim)

    query_heads = heads_of(0)
    key_heads = heads_of(1) * head_dim ** (-0.5)
    value_heads = heads_of(2)
    out_gate = heads_of(3)
    gate_pre = jnp.einsum("sd,gdh->gsh", normed, w_gates, preferred_element_type=jnp.float32)
    gate_pre = gate_pre + gate_bias[:, None, :]
    carried = jax.nn.log_sigmoid(gate_pre[1]) + state_max
    new_max = jnp.maximum(carried, gate_pre[0])
    forget_weight = jnp.exp(carried - new_max)[..., None]
    input_weight = jnp.exp(gate_pre[0] - new_max)[..., None]
    new_norm = forget_weight * state_norm + input_weight * key_heads
    new_matrix = (
        forget_weight[..., None] * state_matrix
        + (input_weight * value_heads)[..., :, None] * key_heads[..., None, :]
    )
    numerator = jnp.einsum(
        "shek,shk->she", new_matrix, query_heads, precision=lax.Precision.HIGHEST
    )
    denominator = jnp.maximum(jnp.abs(jnp.sum(new_norm * query_heads, -1)), 1.0)
    gated_out = (jax.nn.sigmoid(out_gate) * numerator / denominator[..., None]).reshape(
        seq_rows, head_cols
    )
    gated_out = gated_out.astype(jnp.bfloat16)
    mixed_part = jnp.dot(gated_out, w_mix_out, preferred_element_type=jnp.float32)
    mixed_own = lax.psum_scatter(
        mixed_part.astype(jnp.bfloat16), "tp", scatter_dimension=1, tiled=True
    ).astype(jnp.float32)
    residual_own = lax.dynamic_slice_in_dim(hidden_in, column_index * slice_width, slice_width, 1)
    stream_own = (residual_own.astype(jnp.float32) + mixed_own).astype(jnp.bfloat16)
    stream = lax.all_gather(stream_own, "tp", axis=1, tiled=True)
    ffn_in = rms_scale(stream, ffn_gain).astype(jnp.bfloat16)
    shared_hidden = (
        jax.nn.silu(jnp.dot(ffn_in, shared_gate, preferred_element_type=jnp.float32))
        * jnp.dot(ffn_in, shared_up, preferred_element_type=jnp.float32)
    ).astype(jnp.bfloat16)
    shared_part = jnp.dot(shared_hidden, shared_down, preferred_element_type=jnp.float32)
    own_routes = lax.dynamic_slice_in_dim(routes, group_index * seq_rows, seq_rows, 0)
    slot_ids = own_routes * capacity + slot_ranks(own_routes, expert_total)
    slot_range = jnp.arange(expert_total * capacity, dtype=jnp.int32)
    matches = slot_ids[:, :, None] == slot_range[None, None, :]
    chooser = jnp.any(matches, 1).astype(jnp.bfloat16)
    outgoing = jnp.einsum("sj,sd->jd", chooser, ffn_in, preferred_element_type=jnp.float32)
    outgoing = outgoing.astype(jnp.bfloat16).reshape(expert_total, capacity, width)
    arrived = lax.all_to_all(outgoing, "ep", split_axis=0, concat_axis=1, tiled=True)
    gate_values = jnp.einsum(
        "erd,edf->erf", arrived, expert_gate, preferred_element_type=jnp.float32
    )
    up_values = jnp.einsum("erd,edf->erf", arrived, expert_up, preferred_element_type=jnp.float32)
    expert_hidden = (jax.nn.silu(gate_values) * up_values).astype(jnp.bfloat16)
    expert_part = jnp.einsum(
        "erf,efd->erd", expert_hidden, expert_down, preferred_element_type=jnp.float32
    )
    expert_part = expert_part.reshape(local_experts * slot_count, width)
    routed_sum, shared_sum = (
        lax.psum_scatter(
            expert_part.astype(jnp.bfloat16), "tp", scatter_dimension=1, tiled=True
        ).astype(jnp.float32),
        lax.psum_scatter(
            shared_part.astype(jnp.bfloat16), "tp", scatter_dimension=1, tiled=True
        ).astype(jnp.float32),
    )
    expert_rows = routed_sum.astype(jnp.bfloat16)
    returned = lax.all_to_all(
        expert_rows.reshape(local_experts, slot_count, slice_width),
        "ep",
        split_axis=1,
        concat_axis=0,
        tiled=True,
    )
    returned = returned.reshape(expert_total * capacity, slice_width)
    weights = jnp.sum(jnp.where(matches, route_weights[:, :, None], 0.0), 1)
    routed = jnp.dot(weights, returned.astype(jnp.float32), precision=lax.Precision.HIGHEST)
    result = (stream_own.astype(jnp.float32) + shared_sum + routed).astype(jnp.bfloat16)
    return (result, new_matrix, new_norm, new_max)


def solution(mesh):
    placed = (
        P("ep", None),
        P(),
        P("ep", "tp"),
        P("ep", "tp"),
        P("ep", "tp"),
        P("ep", "tp"),
        P(None, None, "tp"),
        P(None, "tp"),
        P("ep", "tp", None, None),
        P("ep", "tp", None),
        P("ep", "tp"),
        P("tp", None),
        P(),
        P(),
        P("ep", None),
        P("ep", None, "tp"),
        P("ep", None, "tp"),
        P("ep", "tp", None),
        P(None, "tp"),
        P(None, "tp"),
        P("tp", None),
    )
    return jax.shard_map(
        per_device,
        mesh=mesh,
        in_specs=placed,
        out_specs=(P("ep", "tp"), P("ep", "tp", None, None), P("ep", "tp", None), P("ep", "tp")),
        check_vma=False,
    )
```

profile of v0, /device:TPU:0, one launch (start us, length us, event | category | flops | bytes accessed | tf_op | source)
XLA Modules:
  0.0 207.5 jit_solution(7990342096338553955)
XLA Ops:
  7.2 0.0 copy-start
  7.2 1.3 fusion.19
  8.4 1.1 fusion.21
  9.5 0.7 copy.88
  10.3 5.2 %all-to-all-start = ((bf16[32,4,1024]{2,0,1:T(8,128)(2,1)}), bf16[32,4,1024]{2,0,1:T(8,128)(2,1)S(1)}, u32[]{:S(2)}, u32[]{:S(2)}) async-start(bf16[32,4,1024]{2,0,1:T(8,128)(2,1)} %bitcast.53), calls=%async_computation | async-start | bytes 524288 | tf_op jit(solution)/shard_map/all_to_all | solution.py:58
  15.5 1.0 fusion.14
  16.5 4.3 %all-to-all-done = bf16[32,4,1024]{2,0,1:T(8,128)(2,1)S(1)} async-done(((bf16[32,4,1024]{2,0,1:T(8,128)(2,1)}), bf16[32,4,1024]{2,0,1:T(8,128)(2,1)S(1)}, u32[]{:S(2)}, u32[]{:S(2)}) %all-to-all-start) | async-done | bytes 262176 | tf_op jit(solution)/shard_map/all_to_all | solution.py:58
  20.8 2.7 %fusion.8 = bf16[128,1024]{1,0:T(8,128)(2,1)} fusion(bf16[128,1024]{1,0:T(8,128)(2,1)S(1)} %bitcast.60, bf16[1024,256]{1,0:T(8,128)(2,1)} %param.26, bf16[1024,256]{1,0:T(8,128)(2,1)} %param.25, bf16[1024,256]{1,0:T(8,128)(2,1)} %param.24, bf16[1024,256]{1,0:T(8,128)(2,1)} %param.23), kind=kOutput, calls=%fused_computation.13 | convolution fusion | flops 276955136 | bytes 2621440 | tf_op jit(solution)/shard_map/dot_general | solution.py:61
  23.5 0.0 reduce-scatter.5.cloned.1.call-update
  23.6 0.0 reduce-scatter.7.cloned.1.call-start
  23.6 0.0 copy-start.5
  23.7 0.1 copy.67
  23.8 0.1 copy.68
  23.8 0.1 copy.70
  23.9 0.1 constant_dynamic-slice_fusion
  24.0 0.1 copy.80
  24.1 0.1 eq.28
  24.2 23.9 %reduce-scatter.5.cloned.1.call-done = bf16[32,1024]{1,0:T(8,128)(2,1)} async-done(((bf16[128,1024]{1,0:T(8,128)(2,1)}), bf16[32,1024]{1,0:T(8,128)(2,1)}) %reduce-scatter.5.cloned.1.call-update) | async-done | bytes 65552 | tf_op jit(solution)/shard_map/reduce_scatter | solution.py:60
  48.1 0.8 fusion.54
  48.9 0.1 reshape.97
  49.0 0.1 reshape.111
  49.1 0.1 reshape.104
  49.2 0.1 reshape.106
  49.3 0.8 multiply_reduce_fusion
  50.1 0.7 add_divide_fusion
  50.8 0.1 div.30
  50.9 3.7 %multiply_add_fusion = f32[32,4,64,64]{3,2,1,0:T(8,128)S(1)} fusion(f32[32,4,64,64]{3,2,1,0:T(8,128)} %param.29, f32[32,4,64]{2,1,0:T(4,128)S(1)} %get-tuple-element.9, f32[32,4,64]{2,1,0:T(4,128)S(1)} %get-tuple-element.13, f32[32,4]{1,0:T(8,128)S(1)} %copy.67), kind=kLoop, calls=%fused_computation.4 | loop fusion | flops 1572864 | bytes 4260352 | tf_op jit(solution)/shard_map/add | solution.py:84
  54.7 2.0 copy-done.1
  56.7 3.4 %fusion.55 = f32[32,4,1,64]{3,2,1,0:T(1,128)S(1)} fusion(f32[32,4,64,64]{3,2,1,0:T(8,128)S(1)} %multiply_add_fusion, bf16[32,4,64,1]{2,3,1,0:T(2,128)(2,1)S(1)} %reshape.111), kind=kOutput, calls=%fused_computation.85 | convolution fusion | flops 6291456 | bytes 2146304 | tf_op jit(solution)/shard_map/shek,shk->she/dot_general | solution.py:87
  60.0 0.1 fusion.31
  60.1 0.1 convert_element_type.79
  60.3 1.2 convolution_convert_fusion.3
  61.4 0.0 reduce-scatter.7.cloned.1.call-update
  61.4 0.0 reduce-scatter.11.cloned.1.call-start
  61.5 0.1 fusion.34
  61.6 0.1 reduce_window_sum.11
  61.7 0.2 select_reduce_fusion.1
  61.8 0.1 reshape.99
  62.0 0.1 copy.72
  62.0 0.1 fusion.33
  62.1 30.2 %reduce-scatter.7.cloned.1.call-done = bf16[32,512]{1,0:T(8,128)(2,1)} async-done(((bf16[32,4096]{1,0:T(8,128)(2,1)}), bf16[32,512]{1,0:T(8,128)(2,1)}) %reduce-scatter.7.cloned.1.call-update) | async-done | bytes 32784 | tf_op jit(solution)/shard_map/reduce_scatter | solution.py:96
  92.3 0.8 add_convert_fusion
  93.1 14.2 %all_gather.3 = bf16[32,4096]{1,0:T(8,128)(2,1)S(1)} all-gather(bf16[32,512]{1,0:T(8,128)(2,1)S(1)} %add_convert_fusion), channel_id=1, replica_groups=mesh['ep'=4,'tp'=8] {'tp'}, dimensions={1}, use_global_device_ids=true | all-gather | bytes 294912 | tf_op jit(solution)/shard_map/all_gather | solution.py:101
  107.3 0.2 fusion.22
  107.5 1.2 convolution_convert_fusion.1
  108.7 1.3 reshape.100
  110.0 18.2 %all_to_all.52 = bf16[8,9,4096]{2,1,0:T(8,128)(2,1)S(1)} all-to-all(bf16[8,9,4096]{2,1,0:T(8,128)(2,1)S(1)} %reshape.100), channel_id=1, replica_groups=mesh['ep'=4,'tp'=8] {'ep'}, dimensions={0} | all-to-all | bytes 1179648 | tf_op jit(solution)/shard_map/all_to_all | solution.py:115
  128.2 0.6 copy.73
  128.8 3.1 %fusion.17 = f32[2,36,256]{2,1,0:T(8,128)S(1)} fusion(bf16[2,4096,256]{2,1,0:T(8,128)(2,1)} %param.36, bf16[2,36,4096]{2,0,1:T(2,128)(2,1)S(1)} %bitcast.54), kind=kOutput, calls=%fused_computation.27 | convolution fusion | flops 150994944 | bytes 4857856 | tf_op jit(solution)/shard_map/erd,edf->erf/dot_general | solution.py:116
  131.9 6.0 %convolution_convert_fusion = bf16[2,36,4096]{2,1,0:T(8,128)(2,1)} fusion(bf16[2,256,4096]{2,1,0:T(8,128)(2,1)} %param.38, bf16[2,4096,256]{2,1,0:T(8,128)(2,1)} %param.37, bf16[2,36,4096]{2,0,1:T(2,128)(2,1)S(1)} %bitcast.55, f32[2,36,256]{2,1,0:T(8,128)S(1)} %fusion.17), kind=kOutput, calls=%fused_computation | convolution fusion | flops 302395392 | bytes 9641984 | tf_op jit(solution)/shard_map/erf,efd->erd/dot_general | solution.py:121
  137.9 2.0 convert_element_type.93
  140.0 0.0 reduce-scatter.11.cloned.1.call-update
  140.0 0.0 reduce-scatter.9.cloned.1.call-start
  140.0 1.6 fusion.51
  141.6 2.9 %convolution_convert_fusion.2 = bf16[32,4096]{1,0:T(8,128)(2,1)} fusion(bf16[128,4096]{1,0:T(8,128)(2,1)} %param.41, bf16[4096,128]{1,0:T(8,128)(2,1)} %param.40, f32[32,128]{1,0:T(8,128)S(1)} %fusion.51, bf16[32,4096]{1,0:T(8,128)(2,1)S(1)} %all_gather.3, f32[4096]{0:T(1024)S(1)} %copy-done.2, f32[32]{0:T(128)S(1)} %add_rsqrt_fusion), kind=kOutput, calls=%fused_computation.2 | convolution fusion | flops 67788800 | bytes 2654336 | tf_op jit(solution)/shard_map/dot_general | solution.py:107
  144.5 0.0 reduce-scatter.9.cloned.1.call-update
  144.5 23.9 %reduce-scatter.11.cloned.1.call-done = bf16[72,512]{1,0:T(8,128)(2,1)} async-done(((bf16[72,4096]{1,0:T(8,128)(2,1)}), bf16[72,512]{1,0:T(8,128)(2,1)}) %reduce-scatter.11.cloned.1.call-update) | async-done | bytes 73744 | tf_op jit(solution)/shard_map/reduce_scatter | solution.py:126
  168.4 0.9 reshape.101
  169.3 0.7 copy.76
  170.0 3.6 %all-to-all-start.2 = ((bf16[2,36,512]{2,0,1:T(2,128)(2,1)}), bf16[2,36,512]{2,0,1:T(2,128)(2,1)S(1)}, u32[]{:S(2)}, u32[]{:S(2)}) async-start(bf16[2,36,512]{2,0,1:T(2,128)(2,1)} %copy.76), calls=%async_computation.6 | async-start | bytes 147456 | tf_op jit(solution)/shard_map/all_to_all | solution.py:134
  173.6 0.1 select_reduce_fusion
  173.7 4.8 %all-to-all-done.2 = bf16[2,36,512]{2,0,1:T(2,128)(2,1)S(1)} async-done(((bf16[2,36,512]{2,0,1:T(2,128)(2,1)}), bf16[2,36,512]{2,0,1:T(2,128)(2,1)S(1)}, u32[]{:S(2)}, u32[]{:S(2)}) %all-to-all-start.2) | async-done | bytes 73760 | tf_op jit(solution)/shard_map/all_to_all | solution.py:134
  178.5 20.9 %reduce-scatter.9.cloned.1.call-done = bf16[32,512]{1,0:T(8,128)(2,1)} async-done(((bf16[32,4096]{1,0:T(8,128)(2,1)}), bf16[32,512]{1,0:T(8,128)(2,1)}) %reduce-scatter.9.cloned.1.call-update) | async-done | bytes 32784 | tf_op jit(solution)/shard_map/reduce_scatter | solution.py:129
  199.4 1.5 fusion.12
  (22 shorter events, 0.2 us)
Async XLA Ops:
  7.2 53.1 %copy-start = (bf16[256,4096]{1,0:T(8,128)(2,1)S(1)}, bf16[256,4096]{1,0:T(8,128)(2,1)}, u32[]{:S(2)}) copy-start(bf16[256,4096]{1,0:T(8,128)(2,1)} %param.32) | copy-start | bytes 6291460
  10.3 10.6 %all-to-all-start = ((bf16[32,4,1024]{2,0,1:T(8,128)(2,1)}), bf16[32,4,1024]{2,0,1:T(8,128)(2,1)S(1)}, u32[]{:S(2)}, u32[]{:S(2)}) async-start(bf16[32,4,1024]{2,0,1:T(8,128)(2,1)} %bitcast.53), calls=%async_computation | async-start | bytes 524288 | tf_op jit(solution)/shard_map/all_to_all | solution.py:58
  15.5 32.7 %reduce-scatter.5.cloned.1.call-start = ((), (), s32[]{:S(2)}) async-start(), calls=%async_computation.7 | async-start | bytes 327680 | tf_op jit(solution)/shard_map/reduce_scatter | solution.py:60
  16.5 7.1 %copy-start.4 = (f32[32,4]{0,1:T(4,128)S(1)}, f32[32,4]{0,1:T(4,128)}, u32[]{:S(2)}) copy-start(f32[32,4]{0,1:T(4,128)} %param.31) | copy-start | bytes 1540
  20.8 3.1 %copy-start.7 = (s32[128,2]{0,1:T(2,128)S(1)}, s32[128,2]{0,1:T(2,128)}, u32[]{:S(2)}) copy-start(s32[128,2]{0,1:T(2,128)} %param.34) | copy-start | bytes 3076
  20.8 28.4 %copy-start.3 = (f32[32,4,64]{2,1,0:T(4,128)S(1)}, f32[32,4,64]{2,1,0:T(4,128)}, u32[]{:S(2)}) copy-start(f32[32,4,64]{2,1,0:T(4,128)} %param.30) | copy-start | bytes 98308
  23.6 68.8 %reduce-scatter.7.cloned.1.call-start = ((), (), s32[]{:S(2)}) async-start(), calls=%async_computation.8 | async-start | bytes 294912 | tf_op jit(solution)/shard_map/reduce_scatter | solution.py:96
  23.6 31.0 %copy-start.5 = (f32[32,4]{0,1:T(4,128)}, f32[32,4]{0,1:T(4,128)S(1)}, u32[]{:S(2)}) copy-start(f32[32,4]{0,1:T(4,128)S(1)} %get-tuple-element.8) | copy-start | bytes 1540
  54.6 2.0 copy-start.1
  56.7 50.8 %copy-start.2 = (f32[4096]{0:T(1024)S(1)}, f32[4096]{0:T(1024)}, u32[]{:S(2)}) copy-start(f32[4096]{0:T(1024)} %param.33) | copy-start | bytes 49156
  61.4 106.9 %reduce-scatter.11.cloned.1.call-start = ((), (), s32[]{:S(2)}) async-start(), calls=%async_computation.10 | async-start | bytes 663552 | tf_op jit(solution)/shard_map/reduce_scatter | solution.py:126
  137.9 35.7 %copy-start.6 = (f32[32,2]{0,1:T(2,128)S(1)}, f32[32,2]{0,1:T(2,128)}, u32[]{:S(2)}) copy-start(f32[32,2]{0,1:T(2,128)} %param.35) | copy-start | bytes 772
  140.0 59.4 %reduce-scatter.9.cloned.1.call-start = ((), (), s32[]{:S(2)}) async-start(), calls=%async_computation.9 | async-start | bytes 294912 | tf_op jit(solution)/shard_map/reduce_scatter | solution.py:129
  170.0 8.5 %all-to-all-start.2 = ((bf16[2,36,512]{2,0,1:T(2,128)(2,1)}), bf16[2,36,512]{2,0,1:T(2,128)(2,1)S(1)}, u32[]{:S(2)}, u32[]{:S(2)}) async-start(bf16[2,36,512]{2,0,1:T(2,128)(2,1)} %copy.76), calls=%async_computation.6 | async-start | bytes 147456 | tf_op jit(solution)/shard_map/all_to_all | solution.py:134
Sparse Core Ops, SparseCore 0:
  23.7 24.3 reduce-scatter.4
  61.6 30.7 reduce-scatter.6
  140.1 28.2 reduce-scatter.10
  170.5 28.9 reduce-scatter.8
where the time goes:
time: 208 us
  waiting for transfers between devices  108 us (52%)
  blocking collectives  32.4 us (16%)
  matrix products  24.5 us (12%)
  between operations  14 us (7%)
  other arithmetic  10 us (5%)
  local copies, waits for them, and re-layouts  9.69 us (5%)
  starting transfers between devices  8.96 us (4%)
    reduce_scatter x1, waiting for transfers between devices, per_device(): lax.psum_scatter(mixed_part.astype(jnp.bfloat16), 'tp', scatter_dimension...  30.2 us
    reduce_scatter x1, waiting for transfers between devices, per_device(): lax.psum_scatter(jnp.dot(gathered, joined, preferred_element_type=jnp.flo...  23.9 us
    reduce_scatter x1, waiting for transfers between devices, per_device(): lax.psum_scatter(expert_part.astype(jnp.bfloat16), 'tp', scatter_dimensio...  23.9 us
    reduce_scatter x1, waiting for transfers between devices, per_device(): lax.psum_scatter(shared_part.astype(jnp.bfloat16), 'tp', scatter_dimensio...  20.9 us
    all_to_all x1, blocking collectives, per_device(): lax.all_to_all(outgoing, 'ep', split_axis=0, concat_axis=1, tiled=True)  18.2 us
    all_gather x1, blocking collectives, per_device(): stream = lax.all_gather(stream_own, 'tp', axis=1, tiled=True)  14.2 us
    dot_general x1, matrix products, per_device(): jnp.einsum('erf,efd->erd', expert_hidden, expert_down, preferred_element_...  6.02 us
    all_to_all x1, starting transfers between devices, per_device(): lax.all_to_all(normed, 'ep', split_axis=1, concat_axis=0, tiled=True)  5.19 us
  transfers between devices with their start and end apart: 6, of which 6 were waited for; matrix products, arithmetic and copies ran while one was open for 4% of the time, Pallas kernels for 0%

commit v1 on v0

--- a/solution.py
+++ b/solution.py
@@ -98,7 +98,12 @@
     ).astype(jnp.float32)
     residual_own = lax.dynamic_slice_in_dim(hidden_in, column_index * slice_width, slice_width, 1)
     stream_own = (residual_own.astype(jnp.float32) + mixed_own).astype(jnp.bfloat16)
-    stream = lax.all_gather(stream_own, "tp", axis=1, tiled=True)
+    ring = [stream_own]
+    for hop in range(7):
+        ring.append(lax.ppermute(ring[-1], "tp", [(dev, (dev + 1) % 8) for dev in range(8)]))
+    stream = jnp.roll(
+        jnp.concatenate(ring[::-1], axis=1), (lax.axis_index("tp") + 1) * ring[0].shape[1], axis=1
+    )
     ffn_in = rms_scale(stream, ffn_gain).astype(jnp.bfloat16)
     shared_hidden = (
         jax.nn.silu(jnp.dot(ffn_in, shared_gate, preferred_element_type=jnp.float32))

time: 208 us -> 224 us (1.077)
  waiting for transfers between devices: 108 us -> 139 us
  blocking collectives: 32.4 us -> 24.6 us
  starting transfers between devices: 8.96 us -> 3.87 us
    ppermute x0 -> x7, waiting for transfers between devices: none -> 35 us  [per_device(): lax.ppermute(ring[-1], 'tp', [(dev, (dev + 1) % 8) for dev in range(8)])]
    all_gather x1 -> x0, blocking collectives: 14.2 us -> none  [per_device(): stream = lax.all_gather(stream_own, 'tp', axis=1, tiled=True)]
    all_to_all x0 -> x1, blocking collectives: none -> 10.7 us  [per_device(): lax.all_to_all(normed, 'ep', split_axis=1, concat_axis=0, tiled=True)]
    all_to_all x1 -> x0, starting transfers between devices: 5.19 us -> none  [per_device(): lax.all_to_all(normed, 'ep', split_axis=1, concat_axis=0, tiled=True)]
    all_to_all x1, blocking collectives: 18.2 us -> 13.8 us  [per_device(): lax.all_to_all(outgoing, 'ep', split_axis=0, concat_axis=1, tiled=True)]
    all_to_all x1 -> x0, waiting for transfers between devices: 4.33 us -> none  [per_device(): lax.all_to_all(normed, 'ep', split_axis=1, concat_axis=0, tiled=True)]
  transfers between devices with their start and end apart: 6 -> 12, of which waited for: 6 -> 12; matrix products, arithmetic and copies ran while one was open for 4% -> 3% of each run, Pallas kernels for 0% -> 0%
where the time goes in v1:
time: 224 us; the launch traced here: 223 us
  waiting for transfers between devices  139 us (62%)
  blocking collectives  24.6 us (11%)
  matrix products  23.1 us (10%)
  between operations  14.1 us (6%)
  other arithmetic  10 us (4%)
  local copies, waits for them, and re-layouts  8.55 us (4%)
  starting transfers between devices  3.87 us (2%)
    ppermute x7, waiting for transfers between devices, per_device(): lax.ppermute(ring[-1], 'tp', [(dev, (dev + 1) % 8) for dev in range(8)])  35 us
    reduce_scatter x1, waiting for transfers between devices, per_device(): lax.psum_scatter(mixed_part.astype(jnp.bfloat16), 'tp', scatter_dimension...  30.9 us
    reduce_scatter x1, waiting for transfers between devices, per_device(): lax.psum_scatter(expert_part.astype(jnp.bfloat16), 'tp', scatter_dimensio...  23.6 us
    reduce_scatter x1, waiting for transfers between devices, per_device(): lax.psum_scatter(jnp.dot(gathered, joined, preferred_element_type=jnp.flo...  23.6 us
    reduce_scatter x1, waiting for transfers between devices, per_device(): lax.psum_scatter(shared_part.astype(jnp.bfloat16), 'tp', scatter_dimensio...  20.9 us
    all_to_all x1, blocking collectives, per_device(): lax.all_to_all(outgoing, 'ep', split_axis=0, concat_axis=1, tiled=True)  13.8 us
    all_to_all x1, blocking collectives, per_device(): lax.all_to_all(normed, 'ep', split_axis=1, concat_axis=0, tiled=True)  10.7 us
    dot_general x1, matrix products, per_device(): jnp.einsum('erf,efd->erd', expert_hidden, expert_down, preferred_element_...  5.17 us
  transfers between devices with their start and end apart: 12, of which 12 were waited for; matrix products, arithmetic and copies ran while one was open for 3% of the time, Pallas kernels for 0%

profile of v1, /device:TPU:0, one launch (start us, length us, event | category | flops | bytes accessed | tf_op | source)
XLA Modules:
  0.0 223.0 jit_solution(13553378395084504847)
XLA Ops:
  7.2 1.2 fusion.19
  8.5 1.1 fusion.21
  9.6 10.7 %all_to_all.52 = bf16[32,4,1024]{2,0,1:T(8,128)(2,1)S(1)} all-to-all(bf16[32,4,1024]{2,0,1:T(8,128)(2,1)S(1)} %bitcast.58), channel_id=1, replica_groups=mesh['ep'=4,'tp'=8] {'ep'}, dimensions={1} | all-to-all | bytes 524288 | tf_op jit(solution)/shard_map/all_to_all | solution.py:58
  20.3 2.7 %fusion.8 = bf16[128,1024]{1,0:T(8,128)(2,1)} fusion(bf16[128,1024]{1,0:T(8,128)(2,1)S(1)} %bitcast.61, bf16[1024,256]{1,0:T(8,128)(2,1)} %param.26, bf16[1024,256]{1,0:T(8,128)(2,1)} %param.25, bf16[1024,256]{1,0:T(8,128)(2,1)} %param.24, bf16[1024,256]{1,0:T(8,128)(2,1)} %param.23), kind=kOutput, calls=%fused_computation.13 | convolution fusion | flops 276955136 | bytes 2621440 | tf_op jit(solution)/shard_map/dot_general | solution.py:61
  23.1 0.0 reduce-scatter.7.cloned.1.call-start
  23.2 0.2 fusion.14
  23.4 0.1 copy.67
  23.5 0.1 copy.68
  23.6 0.1 copy.70
  23.7 23.6 %reduce-scatter.5.cloned.1.call-done = bf16[32,1024]{1,0:T(8,128)(2,1)} async-done(((bf16[128,1024]{1,0:T(8,128)(2,1)}), bf16[32,1024]{1,0:T(8,128)(2,1)}) %reduce-scatter.5.cloned.1.call-update) | async-done | bytes 65552 | tf_op jit(solution)/shard_map/reduce_scatter | solution.py:60
  47.3 0.8 fusion.54
  48.0 0.1 reshape.97
  48.1 0.1 reshape.111
  48.2 0.1 reshape.104
  48.3 0.1 reshape.106
  48.4 0.8 multiply_reduce_fusion
  49.2 0.7 add_divide_fusion
  50.0 0.1 div.30
  50.0 3.7 %multiply_add_fusion = f32[32,4,64,64]{3,2,1,0:T(8,128)S(1)} fusion(f32[32,4,64,64]{3,2,1,0:T(8,128)} %param.29, f32[32,4,64]{2,1,0:T(4,128)S(1)} %get-tuple-element.9, f32[32,4,64]{2,1,0:T(4,128)S(1)} %get-tuple-element.13, f32[32,4]{1,0:T(8,128)S(1)} %copy.67), kind=kLoop, calls=%fused_computation.4 | loop fusion | flops 1572864 | bytes 4260352 | tf_op jit(solution)/shard_map/add | solution.py:84
  53.8 2.0 copy-done.1
  55.8 3.4 %fusion.55 = f32[32,4,1,64]{3,2,1,0:T(1,128)S(1)} fusion(f32[32,4,64,64]{3,2,1,0:T(8,128)S(1)} %multiply_add_fusion, bf16[32,4,64,1]{2,3,1,0:T(2,128)(2,1)S(1)} %reshape.111), kind=kOutput, calls=%fused_computation.101 | convolution fusion | flops 6291456 | bytes 2146304 | tf_op jit(solution)/shard_map/shek,shk->she/dot_general | solution.py:87
  59.2 0.1 fusion.31
  59.3 0.1 convert_element_type.79
  59.4 1.2 convolution_convert_fusion.3
  60.6 0.0 reduce-scatter.11.cloned.1.call-start
  60.6 30.9 %reduce-scatter.7.cloned.1.call-done = bf16[32,512]{1,0:T(8,128)(2,1)} async-done(((bf16[32,4096]{1,0:T(8,128)(2,1)}), bf16[32,512]{1,0:T(8,128)(2,1)}) %reduce-scatter.7.cloned.1.call-update) | async-done | bytes 32784 | tf_op jit(solution)/shard_map/reduce_scatter | solution.py:96
  91.5 0.8 add_convert_fusion
  92.3 0.1 collective-permute-start
  92.4 5.1 %collective-permute-done = bf16[32,512]{1,0:T(8,128)(2,1)S(1)} collective-permute-done((bf16[32,512]{1,0:T(8,128)(2,1)S(1)}, bf16[32,512]{1,0:T(8,128)(2,1)S(1)}, u32[]{:S(2)}, u32[]{:S(2)}) %collective-permute-start) | collective-permute-done | bytes 32800 | tf_op jit(solution)/shard_map/ppermute | solution.py:103
  97.5 5.1 %collective-permute-done.1 = bf16[32,512]{1,0:T(8,128)(2,1)S(1)} collective-permute-done((bf16[32,512]{1,0:T(8,128)(2,1)S(1)}, bf16[32,512]{1,0:T(8,128)(2,1)S(1)}, u32[]{:S(2)}, u32[]{:S(2)}) %collective-permute-start.1) | collective-permute-done | bytes 32800 | tf_op jit(solution)/shard_map/ppermute | solution.py:103
  102.6 0.1 constant_dynamic-slice_fusion
  102.7 0.1 copy.80
  102.8 0.1 eq.31
  102.9 4.9 %collective-permute-done.2 = bf16[32,512]{1,0:T(8,128)(2,1)S(1)} collective-permute-done((bf16[32,512]{1,0:T(8,128)(2,1)S(1)}, bf16[32,512]{1,0:T(8,128)(2,1)S(1)}, u32[]{:S(2)}, u32[]{:S(2)}) %collective-permute-start.2) | collective-permute-done | bytes 32800 | tf_op jit(solution)/shard_map/ppermute | solution.py:103
  107.8 0.1 fusion.34
  107.9 0.1 reduce_window_sum.11
  107.9 5.0 %collective-permute-done.3 = bf16[32,512]{1,0:T(8,128)(2,1)S(1)} collective-permute-done((bf16[32,512]{1,0:T(8,128)(2,1)S(1)}, bf16[32,512]{1,0:T(8,128)(2,1)S(1)}, u32[]{:S(2)}, u32[]{:S(2)}) %collective-permute-start.3) | collective-permute-done | bytes 32800 | tf_op jit(solution)/shard_map/ppermute | solution.py:103
  112.9 0.2 select_reduce_fusion.1
  113.1 0.1 reshape.99
  113.2 4.8 %collective-permute-done.4 = bf16[32,512]{1,0:T(8,128)(2,1)S(1)} collective-permute-done((bf16[32,512]{1,0:T(8,128)(2,1)S(1)}, bf16[32,512]{1,0:T(8,128)(2,1)S(1)}, u32[]{:S(2)}, u32[]{:S(2)}) %collective-permute-start.4) | collective-permute-done | bytes 32800 | tf_op jit(solution)/shard_map/ppermute | solution.py:103
  118.1 0.1 copy.72
  118.1 5.0 %collective-permute-done.5 = bf16[32,512]{1,0:T(8,128)(2,1)S(1)} collective-permute-done((bf16[32,512]{1,0:T(8,128)(2,1)S(1)}, bf16[32,512]{1,0:T(8,128)(2,1)S(1)}, u32[]{:S(2)}, u32[]{:S(2)}) %collective-permute-start.5) | collective-permute-done | bytes 32800 | tf_op jit(solution)/shard_map/ppermute | solution.py:103
  123.2 0.1 fusion.33
  123.3 5.0 %collective-permute-done.6 = bf16[32,512]{1,0:T(8,128)(2,1)S(1)} collective-permute-done((bf16[32,512]{1,0:T(8,128)(2,1)S(1)}, bf16[32,512]{1,0:T(8,128)(2,1)S(1)}, u32[]{:S(2)}, u32[]{:S(2)}) %collective-permute-start.6) | collective-permute-done | bytes 32800 | tf_op jit(solution)/shard_map/ppermute | solution.py:103
  128.5 0.2 fusion.22
  128.7 0.6 copy-done.2
  129.3 1.2 convolution_convert_fusion.1
  130.5 1.3 reshape.100
  131.8 13.8 %all_to_all.53 = bf16[8,9,4096]{2,1,0:T(8,128)(2,1)S(1)} all-to-all(bf16[8,9,4096]{2,1,0:T(8,128)(2,1)S(1)} %reshape.100), channel_id=1, replica_groups=mesh['ep'=4,'tp'=8] {'ep'}, dimensions={0} | all-to-all | bytes 1179648 | tf_op jit(solution)/shard_map/all_to_all | solution.py:120
  145.7 0.6 copy.73
  146.3 3.1 %fusion.17 = f32[2,36,256]{2,1,0:T(8,128)S(1)} fusion(bf16[2,4096,256]{2,1,0:T(8,128)(2,1)} %param.36, bf16[2,36,4096]{2,0,1:T(2,128)(2,1)S(1)} %bitcast.54), kind=kOutput, calls=%fused_computation.27 | convolution fusion | flops 150994944 | bytes 4857856 | tf_op jit(solution)/shard_map/erd,edf->erf/dot_general | solution.py:121
  149.4 5.2 %convolution_convert_fusion = bf16[2,36,4096]{2,1,0:T(8,128)(2,1)S(1)} fusion(bf16[2,256,4096]{2,1,0:T(8,128)(2,1)} %param.38, bf16[2,4096,256]{2,1,0:T(8,128)(2,1)} %param.37, bf16[2,36,4096]{2,0,1:T(2,128)(2,1)S(1)} %bitcast.55, f32[2,36,256]{2,1,0:T(8,128)S(1)} %fusion.17), kind=kOutput, calls=%fused_computation | convolution fusion | flops 302395392 | bytes 9641984 | tf_op jit(solution)/shard_map/erf,efd->erd/dot_general | solution.py:126
  154.6 0.9 convert_element_type.93
  155.5 0.0 reduce-scatter.9.cloned.1.call-start
  155.6 1.6 fusion.51
  157.3 3.0 %convolution_convert_fusion.2 = bf16[32,4096]{1,0:T(8,128)(2,1)} fusion(bf16[128,4096]{1,0:T(8,128)(2,1)} %param.41, bf16[4096,128]{1,0:T(8,128)(2,1)} %param.40, f32[32,128]{1,0:T(8,128)S(1)} %fusion.51, f32[4096]{0:T(1024)S(1)} %copy-done.3, f32[32]{0:T(128)S(1)} %add_rsqrt_fusion, bf16[32,8192]{1,0:T(8,128)(2,1)} %copy-done.2, s32[]{:T(128)S(6)} %select_n.31), kind=kOutput, calls=%fused_computation.2 | convolution fusion | flops 67788800 | bytes 2654340 | tf_op jit(solution)/shard_map/dot_general | solution.py:112
  160.3 23.6 %reduce-scatter.11.cloned.1.call-done = bf16[72,512]{1,0:T(8,128)(2,1)} async-done(((bf16[72,4096]{1,0:T(8,128)(2,1)}), bf16[72,512]{1,0:T(8,128)(2,1)}) %reduce-scatter.11.cloned.1.call-update) | async-done | bytes 73744 | tf_op jit(solution)/shard_map/reduce_scatter | solution.py:131
  183.9 0.9 reshape.101
  184.8 0.7 copy.76
  185.5 3.6 %all-to-all-start.2 = ((bf16[2,36,512]{2,0,1:T(2,128)(2,1)}), bf16[2,36,512]{2,0,1:T(2,128)(2,1)S(1)}, u32[]{:S(2)}, u32[]{:S(2)}) async-start(bf16[2,36,512]{2,0,1:T(2,128)(2,1)} %copy.76), calls=%async_computation.6 | async-start | bytes 147456 | tf_op jit(solution)/shard_map/all_to_all | solution.py:139
  189.1 0.1 select_reduce_fusion
  189.2 4.8 %all-to-all-done.2 = bf16[2,36,512]{2,0,1:T(2,128)(2,1)S(1)} async-done(((bf16[2,36,512]{2,0,1:T(2,128)(2,1)}), bf16[2,36,512]{2,0,1:T(2,128)(2,1)S(1)}, u32[]{:S(2)}, u32[]{:S(2)}) %all-to-all-start.2) | async-done | bytes 73760 | tf_op jit(solution)/shard_map/all_to_all | solution.py:139
  194.0 20.9 %reduce-scatter.9.cloned.1.call-done = bf16[32,512]{1,0:T(8,128)(2,1)} async-done(((bf16[32,4096]{1,0:T(8,128)(2,1)}), bf16[32,512]{1,0:T(8,128)(2,1)}) %reduce-scatter.9.cloned.1.call-update) | async-done | bytes 32784 | tf_op jit(solution)/shard_map/reduce_scatter | solution.py:134
  214.9 1.5 fusion.12
  (56 shorter events, 0.4 us)
Async XLA Ops:
  7.2 52.2 %copy-start = (bf16[256,4096]{1,0:T(8,128)(2,1)S(1)}, bf16[256,4096]{1,0:T(8,128)(2,1)}, u32[]{:S(2)}) copy-start(bf16[256,4096]{1,0:T(8,128)(2,1)} %param.32) | copy-start | bytes 6291460
  7.2 40.1 %reduce-scatter.5.cloned.1.call-start = ((), (), s32[]{:S(2)}) async-start(), calls=%async_computation.7 | async-start | bytes 327680 | tf_op jit(solution)/shard_map/reduce_scatter | solution.py:60
  20.3 2.8 %copy-start.9 = (bf16[2,4096,4]{1,2,0:T(4,128)(2,1)S(1)}, bf16[2,4096,4]{1,2,0:T(4,128)(2,1)}, u32[]{:S(2)}) copy-start(bf16[2,4096,4]{1,2,0:T(4,128)(2,1)} %param.27) | copy-start | bytes 196612
  20.3 2.8 %copy-start.10 = (f32[2,4]{1,0:T(2,128)S(1)}, f32[2,4]{1,0:T(2,128)}, u32[]{:S(2)}) copy-start(f32[2,4]{1,0:T(2,128)} %param.28) | copy-start | bytes 100
  20.3 3.0 %copy-start.5 = (f32[32,4]{0,1:T(4,128)S(1)}, f32[32,4]{0,1:T(4,128)}, u32[]{:S(2)}) copy-start(f32[32,4]{0,1:T(4,128)} %param.31) | copy-start | bytes 1540
  20.3 28.1 %copy-start.4 = (f32[32,4,64]{2,1,0:T(4,128)S(1)}, f32[32,4,64]{2,1,0:T(4,128)}, u32[]{:S(2)}) copy-start(f32[32,4,64]{2,1,0:T(4,128)} %param.30) | copy-start | bytes 98308
  23.1 68.4 %reduce-scatter.7.cloned.1.call-start = ((), (), s32[]{:S(2)}) async-start(), calls=%async_computation.8 | async-start | bytes 294912 | tf_op jit(solution)/shard_map/reduce_scatter | solution.py:96
  23.4 30.4 %copy-start.6 = (f32[32,4]{0,1:T(4,128)}, f32[32,4]{0,1:T(4,128)S(1)}, u32[]{:S(2)}) copy-start(f32[32,4]{0,1:T(4,128)S(1)} %get-tuple-element.8) | copy-start | bytes 1540
  53.8 2.0 copy-start.1
  55.8 46.8 %copy-start.8 = (s32[128,2]{0,1:T(2,128)S(1)}, s32[128,2]{0,1:T(2,128)}, u32[]{:S(2)}) copy-start(s32[128,2]{0,1:T(2,128)} %param.34) | copy-start | bytes 3076
  55.8 73.5 %copy-start.3 = (f32[4096]{0:T(1024)S(1)}, f32[4096]{0:T(1024)}, u32[]{:S(2)}) copy-start(f32[4096]{0:T(1024)} %param.33) | copy-start | bytes 49156
  60.6 123.3 %reduce-scatter.11.cloned.1.call-start = ((), (), s32[]{:S(2)}) async-start(), calls=%async_computation.10 | async-start | bytes 663552 | tf_op jit(solution)/shard_map/reduce_scatter | solution.py:131
  92.3 5.2 %collective-permute-start = (bf16[32,512]{1,0:T(8,128)(2,1)S(1)}, bf16[32,512]{1,0:T(8,128)(2,1)S(1)}, u32[]{:S(2)}, u32[]{:S(2)}) collective-permute-start(bf16[32,512]{1,0:T(8,128)(2,1)S(1)} %add_convert_fusion), channel_id=1, source_target_pairs={{0,1},{1,2},{2,3},{3,4},{4,5},{5,6},{6,7},{7,0},{8,9},{9,10},{10,1... | collective-permute-start | bytes 98312 | tf_op jit(solution)/shard_map/ppermute | solution.py:103
  97.5 5.1 %collective-permute-start.1 = (bf16[32,512]{1,0:T(8,128)(2,1)S(1)}, bf16[32,512]{1,0:T(8,128)(2,1)S(1)}, u32[]{:S(2)}, u32[]{:S(2)}) collective-permute-start(bf16[32,512]{1,0:T(8,128)(2,1)S(1)} %collective-permute-done), channel_id=1, source_target_pairs={{0,1},{1,2},{2,3},{3,4},{4,5},{5,6},{6,7},{7,0},{8,9},{9,10},{10,1... | collective-permute-start | bytes 98312 | tf_op jit(solution)/shard_map/ppermute | solution.py:103
  102.6 5.1 %collective-permute-start.2 = (bf16[32,512]{1,0:T(8,128)(2,1)S(1)}, bf16[32,512]{1,0:T(8,128)(2,1)S(1)}, u32[]{:S(2)}, u32[]{:S(2)}) collective-permute-start(bf16[32,512]{1,0:T(8,128)(2,1)S(1)} %collective-permute-done.1), channel_id=1, source_target_pairs={{0,1},{1,2},{2,3},{3,4},{4,5},{5,6},{6,7},{7,0},{8,9},{9,10},{10,1... | collective-permute-start | bytes 98312 | tf_op jit(solution)/shard_map/ppermute | solution.py:103
  107.8 5.1 %collective-permute-start.3 = (bf16[32,512]{1,0:T(8,128)(2,1)S(1)}, bf16[32,512]{1,0:T(8,128)(2,1)S(1)}, u32[]{:S(2)}, u32[]{:S(2)}) collective-permute-start(bf16[32,512]{1,0:T(8,128)(2,1)S(1)} %collective-permute-done.2), channel_id=1, source_target_pairs={{0,1},{1,2},{2,3},{3,4},{4,5},{5,6},{6,7},{7,0},{8,9},{9,10},{10,1... | collective-permute-start | bytes 98312 | tf_op jit(solution)/shard_map/ppermute | solution.py:103
  112.9 5.1 %collective-permute-start.4 = (bf16[32,512]{1,0:T(8,128)(2,1)S(1)}, bf16[32,512]{1,0:T(8,128)(2,1)S(1)}, u32[]{:S(2)}, u32[]{:S(2)}) collective-permute-start(bf16[32,512]{1,0:T(8,128)(2,1)S(1)} %collective-permute-done.3), channel_id=1, source_target_pairs={{0,1},{1,2},{2,3},{3,4},{4,5},{5,6},{6,7},{7,0},{8,9},{9,10},{10,1... | collective-permute-start | bytes 98312 | tf_op jit(solution)/shard_map/ppermute | solution.py:103
  118.1 5.1 %collective-permute-start.5 = (bf16[32,512]{1,0:T(8,128)(2,1)S(1)}, bf16[32,512]{1,0:T(8,128)(2,1)S(1)}, u32[]{:S(2)}, u32[]{:S(2)}) collective-permute-start(bf16[32,512]{1,0:T(8,128)(2,1)S(1)} %collective-permute-done.4), channel_id=1, source_target_pairs={{0,1},{1,2},{2,3},{3,4},{4,5},{5,6},{6,7},{7,0},{8,9},{9,10},{10,1... | collective-permute-start | bytes 98312 | tf_op jit(solution)/shard_map/ppermute | solution.py:103
  123.2 5.1 %collective-permute-start.6 = (bf16[32,512]{1,0:T(8,128)(2,1)S(1)}, bf16[32,512]{1,0:T(8,128)(2,1)S(1)}, u32[]{:S(2)}, u32[]{:S(2)}) collective-permute-start(bf16[32,512]{1,0:T(8,128)(2,1)S(1)} %collective-permute-done.5), channel_id=1, source_target_pairs={{0,1},{1,2},{2,3},{3,4},{4,5},{5,6},{6,7},{7,0},{8,9},{9,10},{10,1... | collective-permute-start | bytes 98312 | tf_op jit(solution)/shard_map/ppermute | solution.py:103
  128.5 0.8 copy-start.2
  154.6 34.5 %copy-start.7 = (f32[32,2]{0,1:T(2,128)S(1)}, f32[32,2]{0,1:T(2,128)}, u32[]{:S(2)}) copy-start(f32[32,2]{0,1:T(2,128)} %param.35) | copy-start | bytes 772
  155.5 59.4 %reduce-scatter.9.cloned.1.call-start = ((), (), s32[]{:S(2)}) async-start(), calls=%async_computation.9 | async-start | bytes 294912 | tf_op jit(solution)/shard_map/reduce_scatter | solution.py:134
  185.5 8.5 %all-to-all-start.2 = ((bf16[2,36,512]{2,0,1:T(2,128)(2,1)}), bf16[2,36,512]{2,0,1:T(2,128)(2,1)S(1)}, u32[]{:S(2)}, u32[]{:S(2)}) async-start(bf16[2,36,512]{2,0,1:T(2,128)(2,1)} %copy.76), calls=%async_computation.6 | async-start | bytes 147456 | tf_op jit(solution)/shard_map/all_to_all | solution.py:139
Sparse Core Ops, SparseCore 0:
  23.2 24.0 reduce-scatter.4
  60.7 30.7 reduce-scatter.6
  155.7 28.1 reduce-scatter.10
  186.0 28.8 reduce-scatter.8
